TPU v7x, 32 devices: a whole 2x2x4 slice. The times are simulated.
32 devices in a mesh: sp: 8 (over z, y), tp: 4 (over x, core).
Axes of the slice: x: 2, y: 2, z: 4, core: 2. Of those that a mesh axis runs over, the one named last changes fastest.
Arguments:
- residual: bfloat16 [2048, 2048], P(('sp', 'tp')), may hold values from -6 to 6
- ssm_input: bfloat16 [2048, 2048], P('sp', 'tp'), may hold values from -6 to 6
- pole_real: float32 [128, 64], P('tp'), may hold values from -2 to 0
- pole_imaginary: float32 [128, 64], P('tp'), may hold values from 1 to 100
- step_log: float32 [128], P('tp'), may hold values from -8 to 0
- input_real: float32 [128, 64, 16], P('tp'), may hold values from -1 to 1
- entry_map_quadrature: float32 [128, 64, 16], P('tp'), may hold values from -1 to 1
- output_real: float32 [128, 16, 64], P('tp'), may hold values from -0.5 to 0.5
- output_imaginary: float32 [128, 16, 64], P('tp'), may hold values from -0.5 to 0.5
- added_log_decay: float32 [2048, 128], P('sp', 'tp'), may hold values from -2 to 0
- out_weight: bfloat16 [2048, 2048], P('tp'), may hold values from -0.125 to 0.125
- mix_gain: float32 [2048], replicated, may hold values from 0.1 to 1.9
- gate_weight: bfloat16 [2048, 5632], P('sp', 'tp'), may hold values from -0.125 to 0.125
- up_weight: bfloat16 [2048, 5632], P('sp', 'tp'), may hold values from -0.125 to 0.125
- down_weight: bfloat16 [2048, 5632], P('sp', 'tp'), may hold values from -0.078125 to 0.078125
- pre_gain: float32 [2048], replicated, may hold values from 0.1 to 1.9
- post_gain: float32 [2048], replicated, may hold values from 0.1 to 1.9
Outputs:
- merged: bfloat16 [2048, 2048], P(('sp', 'tp'))
All inputs are finite; a program needn't handle non-finite values.
Results may differ from a plain program's by a relative error of at most 0.017.
Values may be sent and summed in bfloat16 or wider, within the bound.
A program may use at most 128 MiB of HBM per device.

v0:
```python
import functools

import jax
import jax.numpy as jnp
from jax import lax
from jax.experimental import pallas as pl
from jax.experimental.pallas import tpu as pltpu
from jax.sharding import PartitionSpec as P

EPSILON = 1e-06
CHUNKS = 8
LANES = 128
BLOCK = 512
MESH = pl.DeviceIdType.MESH


def rms_scale(values, gain):
    return values * lax.rsqrt(jnp.mean(values * values, axis=-1, keepdims=True) + EPSILON) * gain


def split(values):
    high = values.astype(jnp.bfloat16)
    return high, (values - high.astype(jnp.float32)).astype(jnp.bfloat16)


def dot32(a, b):
    return jnp.dot(a, b, preferred_element_type=jnp.float32)


def times(ar, ai, br, bi):
    return ar * br - ai * bi, ar * bi + ai * br


def greet(barrier, nt):
    place = lax.axis_index("tp")
    for d in range(1, nt):
        pl.semaphore_signal(
            barrier, inc=1, device_id={"tp": lax.rem(place + d, nt)}, device_id_type=MESH
        )


def own_rows(nt, rows):
    own = rows // nt
    return pl.ds(pl.multiple_of(lax.axis_index("tp") * own, own), own)


def scatter_rows(nt, part, landed, sems):
    place = lax.axis_index("tp")
    rows = part.shape[0]
    own = rows // nt
    copies = []
    for d in range(1, nt):
        peer = lax.rem(place + d, nt)
        copy = pltpu.make_async_remote_copy(
            src_ref=part.at[pl.ds(pl.multiple_of(peer * own, own), own)],
            dst_ref=landed.at[d - 1],
            send_sem=sems.at[0, d - 1],
            recv_sem=sems.at[1, d - 1],
            device_id={"tp": peer},
            device_id_type=MESH,
        )
        copy.start()
        copies.append(copy)
    total = part[own_rows(nt, rows), :].astype(jnp.float32)
    for d, copy in enumerate(copies):
        copy.wait()
        total = total + landed[d].astype(jnp.float32)
    return total


def ssm_kernel(
    n,
    nt,
    u,
    mag,
    cr,
    ci,
    er,
    ei,
    rr,
    ri,
    order,
    residual,
    weight,
    mix_gain,
    pre_gain,
    middle,
    out,
    dr,
    di,
    ends,
    send,
    recv,
    start,
    active,
    part,
    landed,
    rows_all,
    send_sem,
    recv_sem,
    tp_sem,
):
    me = lax.axis_index("sp")
    rows, flat = dr.shape
    steps = rows // CHUNKS
    packs, width, wide = er.shape
    block = min(BLOCK, flat)

    barrier = pltpu.get_barrier_semaphore()
    for d in range(1, n):
        pl.semaphore_signal(
            barrier, inc=1, device_id={"sp": lax.rem(me + d, n)}, device_id_type=MESH
        )
    greet(barrier, nt)
    for p in range(packs):
        piece = u[:, p * width : (p + 1) * width]
        for e, dst in ((er, dr), (ei, di)):
            high, low = split(e[p])
            dst[:, p * wide : (p + 1) * wide] = dot32(piece, high) + dot32(piece, low)

    for b in range(0, flat, block):
        at = pl.ds(b, block)
        kr = jnp.broadcast_to(cr[0:1, at], (CHUNKS, block))
        ki = jnp.broadcast_to(ci[0:1, at], (CHUNKS, block))

        def first(j, held):
            pr, pi, sr, si = held
            row = pl.ds(pl.multiple_of(j * CHUNKS, CHUNKS), CHUNKS)
            m = mag[row, at]
            ar, ai = m * kr, m * ki
            pr, pi = times(ar, ai, pr, pi)
            sr, si = times(ar, ai, sr, si)
            return pr, pi, sr + dr[row, at], si + di[row, at]

        zero = jnp.zeros((CHUNKS, block), jnp.float32)
        held = lax.fori_loop(0, steps, first, (zero + 1.0, zero, zero, zero), unroll=2)
        for k in range(4):
            ends[k, :, at] = held[k]

    pr, pi, sr, si = (ends[k, 0:1, :] for k in range(4))
    for c in range(1, CHUNKS):
        ar, ai, br, bi = (ends[k, c : c + 1, :] for k in range(4))
        pr, pi = times(ar, ai, pr, pi)
        sr, si = times(ar, ai, sr, si)
        sr, si = sr + br, si + bi
    for k, item in enumerate((pr, pi, sr, si)):
        send[k : k + 1, :] = item

    pl.semaphore_wait(barrier, n - 1 + nt - 1)
    copies = []
    for d in range(1, n):
        copy = pltpu.make_async_remote_copy(
            src_ref=send,
            dst_ref=recv.at[me],
            send_sem=send_sem.at[d - 1],
            recv_sem=recv_sem.at[d - 1],
            device_id={"sp": lax.rem(me + d, n)},
            device_id_type=MESH,
        )
        copy.start()
        copies.append(copy)
    for copy in copies:
        copy.wait()

    sr = jnp.zeros((1, flat), jnp.float32)
    si = sr
    for k in range(n - 1):
        ar, ai, br, bi = (recv[k, q : q + 1, :] for q in range(4))
        nr, ni = times(ar, ai, sr, si)
        sr = jnp.where(k < me, nr + br, sr)
        si = jnp.where(k < me, ni + bi, si)
    for c in range(CHUNKS):
        start[0, c : c + 1, :] = sr
        start[1, c : c + 1, :] = si
        ar, ai, br, bi = (ends[k, c : c + 1, :] for k in range(4))
        sr, si = times(ar, ai, sr, si)
        sr, si = sr + br, si + bi

    for b in range(0, flat, block):
        at = pl.ds(b, block)
        kr = jnp.broadcast_to(cr[0:1, at], (CHUNKS, block))
        ki = jnp.broadcast_to(ci[0:1, at], (CHUNKS, block))

        def second(j, held):
            row = pl.ds(pl.multiple_of(j * CHUNKS, CHUNKS), CHUNKS)
            m = mag[row, at]
            sr, si = times(m * kr, m * ki, *held)
            sr, si = sr + dr[row, at], si + di[row, at]
            dr[row, at] = sr
            di[row, at] = si
            return sr, si

        lax.fori_loop(0, steps, second, (start[0, :, at], start[1, :, at]), unroll=2)

    for p in range(packs):
        total = None
        for state, read in ((dr, rr), (di, ri)):
            high, low = split(state[:, p * wide : (p + 1) * wide])
            top, rest = split(read[p])
            term = dot32(high, top) + dot32(high, rest) + dot32(low, top)
            total = term if total is None else total + term
        active[:, p * width : (p + 1) * width] = jax.nn.gelu(total).astype(jnp.bfloat16)

    active[...] = dot32(order[...], active[...]).astype(jnp.bfloat16)
    columns = weight.shape[1]
    for b in range(0, columns, BLOCK):
        at = pl.ds(b, BLOCK)
        part[:, at] = dot32(active[...], weight[:, at]).astype(jnp.bfloat16)
    mixed = scatter_rows(nt, part, landed, tp_sem)
    inner = (residual[...].astype(jnp.float32) + rms_scale(mixed, mix_gain[...])).astype(
        jnp.bfloat16
    )
    middle[...] = inner
    own = own_rows(nt, rows)
    rows_all[own, :] = rms_scale(inner.astype(jnp.float32), pre_gain[...]).astype(jnp.bfloat16)
    copies = []
    for d in range(1, nt):
        copy = pltpu.make_async_remote_copy(
            src_ref=rows_all.at[own],
            dst_ref=rows_all.at[own],
            send_sem=tp_sem.at[2, d - 1],
            recv_sem=tp_sem.at[3, d - 1],
            device_id={"tp": lax.rem(lax.axis_index("tp") + d, nt)},
            device_id_type=MESH,
        )
        copy.start()
        copies.append(copy)
    for copy in copies:
        copy.wait()
    out[...] = rows_all[...]


def down_kernel(nt, hidden, weight, middle, gain, out, part, landed, tp_sem):
    barrier = pltpu.get_barrier_semaphore()
    greet(barrier, nt)
    for b in range(0, weight.shape[0], BLOCK):
        at = pl.ds(b, BLOCK)
        part[:, at] = lax.dot_general(
            hidden[...],
            weight[at, :],
            (((1,), (1,)), ((), ())),
            preferred_element_type=jnp.float32,
        ).astype(jnp.bfloat16)
    pl.semaphore_wait(barrier, nt - 1)
    total = scatter_rows(nt, part, landed, tp_sem)
    out[...] = (middle[...].astype(jnp.float32) + 0.5 * rms_scale(total, gain[...])).astype(
        jnp.bfloat16
    )


def branch(
    n,
    nt,
    inputs,
    pole_real,
    pole_imaginary,
    step_log,
    input_real,
    entry_map_quadrature,
    output_real,
    output_imaginary,
    added_log_decay,
    residual,
    out_weight,
    mix_gain,
    pre_gain,
):
    rows, channels = inputs.shape
    columns = out_weight.shape[1]
    groups, states = pole_real.shape
    width = input_real.shape[2]
    flat = groups * states
    step_size = jnp.exp(step_log)[:, None]
    log_size = pole_real * step_size
    angle = pole_imaginary * step_size
    cosine = jnp.cos(angle)
    sine = jnp.sin(angle)
    magnitude = jnp.exp(log_size)
    lift_real = jnp.expm1(log_size) * cosine - 2.0 * jnp.sin(0.5 * angle) ** 2
    lift_imaginary = magnitude * sine
    denominator = pole_real * pole_real + pole_imaginary * pole_imaginary
    ratio_real = (lift_real * pole_real + lift_imaginary * pole_imaginary) / denominator
    ratio_imaginary = (lift_imaginary * pole_real - lift_real * pole_imaginary) / denominator
    bar_real = (
        ratio_real[..., None] * input_real - ratio_imaginary[..., None] * entry_map_quadrature
    )
    bar_imaginary = (
        ratio_real[..., None] * entry_map_quadrature + ratio_imaginary[..., None] * input_real
    )
    pack = LANES // width
    packs = groups // pack
    same = jnp.eye(pack, dtype=jnp.float32)

    def entry(bar):
        bar = bar.reshape(packs, pack, states, width).transpose(0, 1, 3, 2)
        return (bar[:, :, :, None, :] * same[None, :, None, :, None]).reshape(
            packs, pack * width, pack * states
        )

    def read(weight):
        weight = weight.reshape(packs, pack, width, states).transpose(0, 1, 3, 2)
        return (weight[:, :, :, None, :] * same[None, :, None, :, None]).reshape(
            packs, pack * states, pack * width
        )

    def mixed_rows(values):
        return values.reshape(CHUNKS, rows // CHUNKS, -1).transpose(1, 0, 2).reshape(rows, -1)

    spread = jnp.repeat(mixed_rows(jnp.exp(added_log_decay)), states, axis=1)
    vmem = pl.BlockSpec(memory_space=pltpu.VMEM)
    place = jnp.arange(rows)
    order = jax.nn.one_hot(
        place % (rows // CHUNKS) * CHUNKS + place // (rows // CHUNKS), rows, dtype=jnp.bfloat16
    )
    return pl.pallas_call(
        functools.partial(ssm_kernel, n, nt),
        out_shape=(
            jax.ShapeDtypeStruct((rows // nt, columns), jnp.bfloat16),
            jax.ShapeDtypeStruct((rows, columns), jnp.bfloat16),
        ),
        in_specs=[vmem] * 13,
        out_specs=(vmem, vmem),
        scratch_shapes=[
            pltpu.VMEM((rows, flat), jnp.float32),
            pltpu.VMEM((rows, flat), jnp.float32),
            pltpu.VMEM((4, CHUNKS, flat), jnp.float32),
            pltpu.VMEM((CHUNKS, flat), jnp.float32),
            pltpu.VMEM((n, CHUNKS, flat), jnp.float32),
            pltpu.VMEM((2, CHUNKS, flat), jnp.float32),
            pltpu.VMEM((rows, channels), jnp.bfloat16),
            pltpu.VMEM((rows, columns), jnp.bfloat16),
            pltpu.VMEM((nt - 1, rows // nt, columns), jnp.bfloat16),
            pltpu.VMEM((rows, columns), jnp.bfloat16),
            pltpu.SemaphoreType.DMA((n - 1,)),
            pltpu.SemaphoreType.DMA((n - 1,)),
            pltpu.SemaphoreType.DMA((4, nt - 1)),
        ],
        cost_estimate=pl.CostEstimate(
            flops=24000000000, bytes_accessed=8000000, transcendentals=0
        ),
        compiler_params=pltpu.CompilerParams(
            collective_id=0, has_side_effects=True, vmem_limit_bytes=40 * 1024 * 1024
        ),
    )(
        mixed_rows(inputs),
        spread,
        (magnitude * cosine).reshape(1, flat),
        (magnitude * sine).reshape(1, flat),
        entry(bar_real),
        entry(bar_imaginary),
        read(output_real),
        read(-output_imaginary),
        order,
        residual,
        out_weight,
        mix_gain.reshape(1, columns),
        pre_gain.reshape(1, columns),
    )


def shards(
    n,
    nt,
    residual,
    ssm_input,
    pole_real,
    pole_imaginary,
    step_log,
    input_real,
    entry_map_quadrature,
    output_real,
    output_imaginary,
    added_log_decay,
    out_weight,
    mix_gain,
    gate_weight,
    up_weight,
    down_weight,
    pre_gain,
    post_gain,
):
    gate_full, up_full, down_full = (
        lax.all_gather(gate_weight, "sp", axis=0, tiled=True),
        lax.all_gather(up_weight, "sp", axis=0, tiled=True),
        lax.all_gather(down_weight, "sp", axis=0, tiled=True),
    )
    middle, mixer_input = branch(
        n,
        nt,
        ssm_input,
        pole_real,
        pole_imaginary,
        step_log,
        input_real,
        entry_map_quadrature,
        output_real,
        output_imaginary,
        added_log_decay,
        residual,
        out_weight,
        mix_gain,
        pre_gain,
    )
    gate_act = jnp.dot(mixer_input, gate_full, preferred_element_type=jnp.float32)
    up_act = jnp.dot(mixer_input, up_full, preferred_element_type=jnp.float32)
    hidden = (jax.nn.silu(gate_act) * up_act).astype(jnp.bfloat16)
    rows, columns = mixer_input.shape
    return pl.pallas_call(
        functools.partial(down_kernel, nt),
        out_shape=jax.ShapeDtypeStruct(residual.shape, jnp.bfloat16),
        in_specs=[pl.BlockSpec(memory_space=pltpu.VMEM)] * 4,
        out_specs=pl.BlockSpec(memory_space=pltpu.VMEM),
        scratch_shapes=[
            pltpu.VMEM((rows, columns), jnp.bfloat16),
            pltpu.VMEM((nt - 1, rows // nt, columns), jnp.bfloat16),
            pltpu.SemaphoreType.DMA((2, nt - 1)),
        ],
        cost_estimate=pl.CostEstimate(flops=8000000000, bytes_accessed=8000000, transcendentals=0),
        compiler_params=pltpu.CompilerParams(
            collective_id=1, has_side_effects=True, vmem_limit_bytes=24 * 1024 * 1024
        ),
    )(hidden, down_full, middle, post_gain.reshape(1, columns))


def solution(mesh):
    return jax.shard_map(
        functools.partial(shards, mesh.shape["sp"], mesh.shape["tp"]),
        mesh=mesh,
        in_specs=(
            P(("sp", "tp"), None),
            P("sp", "tp"),
            P("tp", None),
            P("tp", None),
            P("tp"),
            P("tp", None, None),
            P("tp", None, None),
            P("tp", None, None),
            P("tp", None, None),
            P("sp", "tp"),
            P("tp", None),
            P(),
            P("sp", "tp"),
            P("sp", "tp"),
            P("sp", "tp"),
            P(),
            P(),
        ),
        out_specs=P(("sp", "tp"), None),
        check_vma=False,
    )
```

profile of v0, /device:TPU:0, one launch (start us, length us, event | category | flops | bytes accessed | tf_op | source)
XLA Modules:
  0.0 323.6 jit_solution(42444697057750321)
XLA Ops:
  6.6 0.7 all-gather.4.cloned.1.call-update
  7.3 0.0 all-gather.6.cloned.1.call-start
  7.3 0.7 all-gather.6.cloned.1.call-update
  8.0 0.0 all-gather.8.cloned.1.call-start
  8.1 0.7 all-gather.8.cloned.1.call-update
  8.8 0.2 fusion.2
  9.0 0.1 multiply_add_fusion
  9.1 0.2 mul.199
  9.4 0.5 mul.200
  9.9 0.2 mul.207
  10.1 1.5 mul.208
  11.6 0.1 copy.24
  11.7 0.1 mul.201
  11.8 0.1 mul.202
  11.9 0.1 reshape.96.cr
  12.0 0.1 reshape.97.ci
  12.1 0.1 mul.212
  12.2 0.1 mul.213
  12.3 0.8 copy.26
  13.2 0.1 copy.28
  13.3 0.2 mul.216
  13.5 1.5 mul.217
  15.1 2.6 copy.29
  17.6 0.1 copy.25
  17.7 0.2 mul.210
  18.0 1.5 mul.211
  19.5 2.7 copy.27
  22.2 0.1 reshape.93
  22.3 0.1 copy.22
  22.4 0.1 copy.23
  22.5 1.5 broadcast_in_dim.3
  24.0 1.9 copy.30.mag
  26.0 1.1 copy.32
  27.1 0.1 fusion.1.order
  27.2 1.7 broadcast_multiply_fusion.2
  29.0 0.1 copy-done.7
  29.1 0.0 copy-done.8
  29.1 0.1 broadcast_multiply_fusion
  29.3 1.4 copy-done.1
  30.7 48.6 %shard_map.163 = (bf16[64,2048]{1,0:T(8,128)(2,1)S(1)}, bf16[256,2048]{1,0:T(8,128)(2,1)S(1)}) custom-call(bf16[256,512]{1,0:T(8,128)(2,1)S(1)} %bitcast.49, f32[256,2048]{1,0:T(8,128)S(1)} %copy.30.mag, f32[1,2048]{1,0:T(1,128)S(1)} %reshape.96.cr, f32[1,2048]{1,0:T(1,128)S(1)} %reshape.97.ci, f32[4,128,512]{2,1,0:T(8,128)S(1)} %get-tuple-element.14.er, ...), custom_call_target="tpu_custom_call" | custom-call | flops 24000000000 | bytes 8000000 | tf_op jit(solution)/shard_map/pallas_call | solution.py:315
  79.3 35.5 %all-gather.4.cloned.1.call-done = bf16[2048,1408]{1,0:T(8,128)(2,1)} async-done(((bf16[256,1408]{1,0:T(8,128)(2,1)}), bf16[2048,1408]{1,0:T(8,128)(2,1)}) %all-gather.4.cloned.1.call-update) | async-done | bytes 5767184 | tf_op jit(solution)/shard_map/all_gather | solution.py:383
  114.8 5.5 %fusion.10 = f32[256,1408]{1,0:T(8,128)} fusion(bf16[256,2048]{1,0:T(8,128)(2,1)S(1)} %get-tuple-element.7, bf16[2048,1408]{1,0:T(8,128)(2,1)} %all-gather.4.cloned.1.call-done), kind=kOutput, calls=%fused_computation.31 | convolution fusion | flops 1476395008 | bytes 8257536 | tf_op jit(solution)/shard_map/dot_general | solution.py:404
  120.3 87.2 %all-gather.6.cloned.1.call-done = bf16[2048,1408]{1,0:T(8,128)(2,1)} async-done(((bf16[256,1408]{1,0:T(8,128)(2,1)}), bf16[2048,1408]{1,0:T(8,128)(2,1)}) %all-gather.6.cloned.1.call-update) | async-done | bytes 5767184 | tf_op jit(solution)/shard_map/all_gather | solution.py:384
  207.5 4.9 %fusion.hidden = bf16[256,1408]{1,0:T(8,128)(2,1)S(1)} fusion(bf16[256,2048]{1,0:T(8,128)(2,1)S(1)} %get-tuple-element.7, bf16[2048,1408]{1,0:T(8,128)(2,1)} %all-gather.6.cloned.1.call-done, f32[256,1408]{1,0:T(8,128)} %fusion.10), kind=kOutput, calls=%fused_computation.1 | convolution fusion | flops 1478557696 | bytes 8978432 | tf_op jit(solution)/shard_map/dot_general | solution.py:405
  212.4 87.9 %all-gather.8.cloned.1.call-done.weight = bf16[2048,1408]{1,0:T(8,128)(2,1)} async-done(((bf16[256,1408]{1,0:T(8,128)(2,1)}), bf16[2048,1408]{1,0:T(8,128)(2,1)}) %all-gather.8.cloned.1.call-update) | async-done | bytes 5767184 | tf_op jit(solution)/shard_map/all_gather | solution.py:385
  300.2 2.6 copy-done
  302.9 13.5 %shard_map.164 = bf16[64,2048]{1,0:T(8,128)(2,1)S(1)} custom-call(bf16[256,1408]{1,0:T(8,128)(2,1)S(1)} %fusion.hidden, bf16[2048,1408]{1,0:T(8,128)(2,1)S(1)} %copy-done, bf16[64,2048]{1,0:T(8,128)(2,1)S(1)} %get-tuple-element.8.middle, f32[1,2048]{1,0:T(1,128)S(1)} %bitcast.52), custom_call_target="tpu_custom_call" | custom-call | flops 8000000000 | bytes 8000000 | tf_op jit(solution)/shard_map/pallas_call | solution.py:408
  316.4 0.7 copy.34
  (36 shorter events, 0.1 us)
Async XLA Ops:
  6.5 2.2 copy-start.16
  6.5 2.3 copy-start.15
  6.5 2.3 copy-start.14
  6.5 2.5 copy-start.11
  6.5 2.5 copy-start.12
  6.5 108.3 %all-gather.4.cloned.1.call-start = ((), (), s32[]{:S(2)}) async-start(), calls=%async_computation | async-start | bytes 6488064 | tf_op jit(solution)/shard_map/all_gather | solution.py:383
  7.3 200.2 %all-gather.6.cloned.1.call-start = ((), (), s32[]{:S(2)}) async-start(), calls=%async_computation.1 | async-start | bytes 6488064 | tf_op jit(solution)/shard_map/all_gather | solution.py:384
  8.0 292.2 %all-gather.8.cloned.1.call-start = ((), (), s32[]{:S(2)}) async-start(), calls=%async_computation.2 | async-start | bytes 6488064 | tf_op jit(solution)/shard_map/all_gather | solution.py:385
  11.6 1.6 copy-start.9
  15.1 2.6 copy-start.10
  18.0 4.2 %copy-start.13 = (f32[256,32]{0,1:T(8,128)S(1)}, f32[256,32]{0,1:T(8,128)}, u32[]{:S(2)}) copy-start(f32[256,32]{0,1:T(8,128)} %param.26) | copy-start | bytes 98308
  27.2 1.8 copy-start.6
  27.2 1.9 copy-start.7
  27.2 1.9 copy-start.8
  29.1 1.6 copy-start.1
  29.1 1.6 copy-start.2
  29.1 1.6 copy-start.3
  29.1 1.6 copy-start.4
  120.3 179.9 %copy-start.5 = (f32[2048]{0:T(1024)S(1)}, f32[2048]{0:T(1024)}, u32[]{:S(2)}) copy-start(f32[2048]{0:T(1024)} %param.33) | copy-start | bytes 24580
  300.2 2.6 copy-start
Sparse Core Ops, SparseCore 0:
  9.5 105.2 all-gather.3
  117.0 90.4 all-gather.5
  209.7 90.4 all-gather.7
where the time goes:
time: 324 us
  waiting for transfers between devices  213 us (66%)
  Pallas kernels  62.1 us (19%)
  local copies, waits for them, and re-layouts  22.8 us (7%)
  between operations  13.4 us (4%)
  matrix products  10.4 us (3%)
    all_gather x1, waiting for transfers between devices, shards(): lax.all_gather(down_weight, 'sp', axis=0, tiled=True)  87.9 us
    all_gather x1, waiting for transfers between devices, shards(): lax.all_gather(up_weight, 'sp', axis=0, tiled=True)  87.2 us
    pallas_call x1, Pallas kernels, branch(): pl.pallas_call(functools.partial(ssm_kernel, n, nt), out_shape=(jax.Shape...  48.6 us
    all_gather x1, waiting for transfers between devices, shards(): lax.all_gather(gate_weight, 'sp', axis=0, tiled=True)  35.5 us
    pallas_call x1, Pallas kernels, shards(): pl.pallas_call(functools.partial(down_kernel, nt), out_shape=jax.ShapeDty...  13.5 us
    mul x9, local copies, waits for them, and re-layouts, read(): weight[:, :, :, None, :] * same[None, :, None, :, None]  9.86 us
  transfers between devices with their start and end apart: 3, of which 3 were waited for; matrix products, arithmetic and copies ran while one was open for 9% of the time, Pallas kernels for 15%

commit v1 on v0

v1 whole, which is shorter than its diff:
```python
import functools
import math

import jax
import jax.numpy as jnp
from jax import lax
from jax.experimental import pallas as pl
from jax.experimental.pallas import tpu as pltpu
from jax.sharding import PartitionSpec as P

EPSILON = 1e-06
CHUNKS = 8
LANES = 128
BLOCK = 512
CORES = 2
MESH = pl.DeviceIdType.MESH


def rms_scale(values, gain):
    return values * lax.rsqrt(jnp.mean(values * values, axis=-1, keepdims=True) + EPSILON) * gain


def split(values):
    high = values.astype(jnp.bfloat16)
    return high, (values - high.astype(jnp.float32)).astype(jnp.bfloat16)


def dot32(a, b):
    return jnp.dot(a, b, preferred_element_type=jnp.float32)


def times(ar, ai, br, bi):
    return ar * br - ai * bi, ar * bi + ai * br


class Links:
    def __init__(self, n, nt, nz):
        self.nz, self.ny, self.nx, self.nc = nz, n // nz, nt // CORES, CORES
        sp, tp = lax.axis_index("sp"), lax.axis_index("tp")
        self.z, self.y = lax.div(sp, self.ny), lax.rem(sp, self.ny)
        self.x, self.c = lax.div(tp, self.nc), lax.rem(tp, self.nc)
        self.sent = []

    def far(self, dz=0, dy=0, dx=0, dc=0):
        return {
            "sp": lax.rem(self.z + dz, self.nz) * self.ny + lax.rem(self.y + dy, self.ny),
            "tp": lax.rem(self.x + dx, self.nx) * self.nc + lax.rem(self.c + dc, self.nc),
        }

    def copy(self, src, dst, sems, index, device):
        made = pltpu.make_async_remote_copy(
            src_ref=src,
            dst_ref=dst,
            send_sem=sems.at[(0,) + index],
            recv_sem=sems.at[(1,) + index],
            device_id=device,
            device_id_type=MESH,
        )
        made.start()
        self.sent.append(made)
        return made


def span(index, size):
    return pl.ds(pl.multiple_of(index * size, size), size)


class Weights:
    def __init__(self, links, sources, held, local, z_sem, x_sem, y_sem, d_sem):
        self.links, self.sources, self.held = links, sources, held
        self.local, self.z_sem, self.x_sem, self.y_sem, self.d_sem = (
            local,
            z_sem,
            x_sem,
            y_sem,
            d_sem,
        )
        self.depth, self.units = sources[0].shape
        self.wide = held.shape[2] // links.nx
        self.coming = {}

    def piece(self, z, x):
        links = self.links
        nt = links.nx * links.nc
        tp = x * links.nc + links.c
        which = lax.rem(z + links.nz * nt - tp - 1, links.nz)
        first = jnp.minimum(which * self.wide, self.units - self.wide)
        return which, pl.multiple_of(first, LANES)

    def spot(self, j, dz, dy, slot):
        links = self.links
        origin = lax.rem(links.z - dz + links.nz, links.nz) * links.ny + lax.rem(
            links.y - dy + links.ny, links.ny
        )
        return self.held.at[j, span(origin, self.depth), pl.ds(slot * self.wide, self.wide)]

    def cut(self, j, dz):
        links = self.links
        _, first = self.piece(lax.rem(links.z + dz, links.nz), links.x)
        return self.sources[j].at[:, pl.ds(first, self.wide)]

    def begin(self):
        links = self.links
        self.own = []
        for j in range(len(self.sources)):
            own = pltpu.make_async_copy(self.cut(j, 0), self.spot(j, 0, 0, 0), self.local.at[j])
            own.start()
            self.own.append(own)

    def along_z(self):
        links = self.links
        for j in range(len(self.sources)):
            for dz in range(1, links.nz):
                self.coming["z", j, dz] = links.copy(
                    self.cut(j, dz), self.spot(j, 0, 0, 0), self.z_sem, (j, dz - 1), links.far(dz=dz)
                )

    def arrive(self, *key):
        made = self.coming.pop(key, None)
        if made is not None:
            made.wait_recv()

    def spread(self, j, zr):
        links = self.links
        if zr == 0:
            self.own[j].wait()
        else:
            self.arrive("z", j, zr)
        here = self.spot(j, zr, 0, 0)
        for dx in range(1, links.nx):
            self.coming["x", j, zr, dx] = links.copy(
                here, self.spot(j, zr, 0, dx), self.x_sem, (j, zr, dx - 1), links.far(dx=dx)
            )
        for dy in range(1, links.ny):
            self.coming["y", j, zr, dy] = links.copy(
                here, here, self.y_sem, (j, zr, dy - 1), links.far(dy=dy)
            )

    def relay(self, j, zr):
        links = self.links
        if (j + zr) % 2 == 0:
            for dx in range(1, links.nx):
                self.arrive("x", j, zr, dx)
                here = self.spot(j, zr, 0, dx)
                for dy in range(1, links.ny):
                    self.coming["d", j, zr, dx, dy] = links.copy(
                        here, here, self.d_sem, (j, zr, dx - 1, dy - 1), links.far(dy=dy)
                    )
        else:
            for dy in range(1, links.ny):
                self.arrive("y", j, zr, dy)
                for dx in range(1, links.nx):
                    self.coming["d", j, zr, dx, dy] = links.copy(
                        self.spot(j, zr, dy, 0),
                        self.spot(j, zr, dy, dx),
                        self.d_sem,
                        (j, zr, dx - 1, dy - 1),
                        links.far(dx=dx),
                    )

    def need(self, j, zr):
        for key in [key for key in self.coming if key[1:3] == (j, zr)]:
            self.arrive(*key)


def layer_kernel(
    n,
    nt,
    nz,
    u,
    mag,
    cr,
    ci,
    er,
    ei,
    rr,
    ri,
    order,
    residual,
    weight,
    mix_gain,
    pre_gain,
    post_gain,
    gate_weight,
    up_weight,
    down_weight,
    out,
    dr,
    di,
    ends,
    send,
    recv,
    start,
    active,
    part,
    pair_land,
    half,
    half_land,
    held,
    rows_all,
    hidden,
    other,
    other_land,
    sums,
    sums_send,
    sums_land,
    send_sem,
    recv_sem,
    local_sem,
    z_sem,
    x_sem,
    y_sem,
    d_sem,
    pair_sem,
    half_sem,
    row_sem,
    row_pair_sem,
    other_sem,
    sums_sem,
):
    me = lax.axis_index("sp")
    links = Links(n, nt, nz)
    nx, nc, ny = links.nx, links.nc, links.ny
    rows, flat = dr.shape
    own = rows // nt
    steps = rows // CHUNKS
    packs, width, wide = er.shape
    block = min(BLOCK, flat)

    barrier = pltpu.get_barrier_semaphore()
    for d in range(1, n):
        pl.semaphore_signal(
            barrier, inc=1, device_id={"sp": lax.rem(me + d, n)}, device_id_type=MESH
        )
    place = lax.axis_index("tp")
    for d in range(1, nt):
        pl.semaphore_signal(
            barrier, inc=1, device_id={"tp": lax.rem(place + d, nt)}, device_id_type=MESH
        )
    weights = Weights(
        links, (gate_weight, up_weight, down_weight), held, local_sem, z_sem, x_sem, y_sem, d_sem
    )
    weights.begin()
    pl.semaphore_wait(barrier, n - 1 + nt - 1)
    weights.along_z()
    for j in range(3):
        weights.spread(j, 0)

    for p in range(packs):
        piece = u[:, p * width : (p + 1) * width]
        for e, dst in ((er, dr), (ei, di)):
            high, low = split(e[p])
            dst[:, p * wide : (p + 1) * wide] = dot32(piece, high) + dot32(piece, low)

    for b in range(0, flat, block):
        at = pl.ds(b, block)
        kr = jnp.broadcast_to(cr[0:1, at], (CHUNKS, block))
        ki = jnp.broadcast_to(ci[0:1, at], (CHUNKS, block))

        def first(j, held_values):
            pr, pi, sr, si = held_values
            row = pl.ds(pl.multiple_of(j * CHUNKS, CHUNKS), CHUNKS)
            m = mag[row, at]
            ar, ai = m * kr, m * ki
            pr, pi = times(ar, ai, pr, pi)
            sr, si = times(ar, ai, sr, si)
            return pr, pi, sr + dr[row, at], si + di[row, at]

        zero = jnp.zeros((CHUNKS, block), jnp.float32)
        values = lax.fori_loop(0, steps, first, (zero + 1.0, zero, zero, zero), unroll=2)
        for k in range(4):
            ends[k, :, at] = values[k]

    pr, pi, sr, si = (ends[k, 0:1, :] for k in range(4))
    for c in range(1, CHUNKS):
        ar, ai, br, bi = (ends[k, c : c + 1, :] for k in range(4))
        pr, pi = times(ar, ai, pr, pi)
        sr, si = times(ar, ai, sr, si)
        sr, si = sr + br, si + bi
    for k, item in enumerate((pr, pi, sr, si)):
        send[k : k + 1, :] = item[:, : flat // 2]
        send[4 + k : 5 + k, :] = item[:, flat // 2 :]

    copies = []
    for d in range(1, n):
        copy = pltpu.make_async_remote_copy(
            src_ref=send,
            dst_ref=recv.at[me],
            send_sem=send_sem.at[d - 1],
            recv_sem=recv_sem.at[d - 1],
            device_id={"sp": lax.rem(me + d, n)},
            device_id_type=MESH,
        )
        pl.when(me + d < n)(copy.start)
        copies.append(copy)

    for j in range(3):
        weights.relay(j, 0)
    for zr in range(1, nz):
        weights.spread(0, zr)

    for d, copy in enumerate(copies, 1):
        pl.when(me >= d)(copy.wait_recv)

    sr = jnp.zeros((1, flat), jnp.float32)
    si = sr
    for k in range(n - 1):
        ar, ai, br, bi = (
            jnp.concatenate([recv[k, q : q + 1, :], recv[k, 4 + q : 5 + q, :]], axis=1)
            for q in range(4)
        )
        nr, ni = times(ar, ai, sr, si)
        sr = jnp.where(k < me, nr + br, sr)
        si = jnp.where(k < me, ni + bi, si)
    for c in range(CHUNKS):
        start[0, c : c + 1, :] = sr
        start[1, c : c + 1, :] = si
        ar, ai, br, bi = (ends[k, c : c + 1, :] for k in range(4))
        sr, si = times(ar, ai, sr, si)
        sr, si = sr + br, si + bi

    for b in range(0, flat, block):
        at = pl.ds(b, block)
        kr = jnp.broadcast_to(cr[0:1, at], (CHUNKS, block))
        ki = jnp.broadcast_to(ci[0:1, at], (CHUNKS, block))

        def second(j, held_values):
            row = pl.ds(pl.multiple_of(j * CHUNKS, CHUNKS), CHUNKS)
            m = mag[row, at]
            sr, si = times(m * kr, m * ki, *held_values)
            sr, si = sr + dr[row, at], si + di[row, at]
            dr[row, at] = sr
            di[row, at] = si
            return sr, si

        lax.fori_loop(0, steps, second, (start[0, :, at], start[1, :, at]), unroll=2)

    for p in range(packs):
        total = None
        for state, read in ((dr, rr), (di, ri)):
            high, low = split(state[:, p * wide : (p + 1) * wide])
            top, rest = split(read[p])
            term = dot32(high, top) + dot32(high, rest) + dot32(low, top)
            total = term if total is None else total + term
        active[:, p * width : (p + 1) * width] = jax.nn.gelu(total).astype(jnp.bfloat16)

    active[...] = dot32(order[...], active[...]).astype(jnp.bfloat16)
    columns = weight.shape[1]
    for b in range(0, columns, BLOCK):
        at = pl.ds(b, BLOCK)
        part[:, at] = dot32(active[...], weight[:, at]).astype(jnp.bfloat16)

    def rows_of(x, c):
        return span(x * nc + c, own)

    pairs = []
    for dc in range(1, nc):
        for x in range(nx):
            pairs.append(
                links.copy(
                    part.at[rows_of(x, lax.rem(links.c + dc, nc))],
                    pair_land.at[dc - 1, x],
                    pair_sem,
                    (dc - 1, x),
                    links.far(dc=dc),
                )
            )
    for zr in range(1, nz):
        weights.relay(0, zr)
    for made in pairs:
        made.wait_recv()

    def chip_sum(x):
        value = part[rows_of(x, links.c), :].astype(jnp.float32)
        for dc in range(1, nc):
            value = value + pair_land[dc - 1, x].astype(jnp.float32)
        return value

    halves = []
    for dx in range(1, nx):
        half[dx - 1] = chip_sum(lax.rem(links.x + dx, nx)).astype(jnp.bfloat16)
        halves.append(
            links.copy(half.at[dx - 1], half_land.at[dx - 1], half_sem, (dx - 1,), links.far(dx=dx))
        )
    mixed = chip_sum(links.x)
    for dx, made in enumerate(halves):
        made.wait_recv()
        mixed = mixed + half_land[dx].astype(jnp.float32)
    middle = (residual[...].astype(jnp.float32) + rms_scale(mixed, mix_gain[...])).astype(
        jnp.bfloat16
    )
    line = nz * own
    mine = span(links.z, own)
    rows_all[mine, :] = rms_scale(middle.astype(jnp.float32), pre_gain[...]).astype(jnp.bfloat16)
    along = []
    for dz in range(1, nz):
        along.append(
            links.copy(rows_all.at[mine], rows_all.at[mine], row_sem, (dz - 1,), links.far(dz=dz))
        )
    to_pair = []

    def hand_over(zr):
        index = lax.rem(links.z - zr + nz, nz)
        for dc in range(1, nc):
            to_pair.append(
                links.copy(
                    rows_all.at[span(index, own)],
                    rows_all.at[span(dc * nz + index, own)],
                    row_pair_sem,
                    (zr, dc - 1),
                    links.far(dc=dc),
                )
            )

    hand_over(0)
    for zr in range(1, nz):
        weights.spread(1, zr)
    for zr in range(1, nz):
        weights.relay(1, zr)
    for zr in range(1, nz):
        weights.spread(2, zr)
    for zr in range(1, nz):
        along[zr - 1].wait_recv()
        hand_over(zr)
    for zr in range(1, nz):
        weights.relay(2, zr)
    for made in to_pair:
        made.wait_recv()
    for j in range(2):
        for zr in range(nz):
            weights.need(j, zr)

    valid = []
    for slot in range(nx):
        which, begin = weights.piece(links.z, lax.rem(links.x - slot + nx, nx))
        at = lax.broadcasted_iota(jnp.int32, (1, weights.wide), 1)
        valid.append(jnp.where(begin + at >= which * weights.wide, 1.0, 0.0))
    valid = jnp.concatenate(valid, axis=1)

    def mix(b, carry):
        at = span(b, line)
        gate = dot32(rows_all[at, :], held[0])
        up = dot32(rows_all[at, :], held[1])
        hidden[at, :] = (jax.nn.silu(gate) * up * valid).astype(jnp.bfloat16)
        return carry

    lax.fori_loop(0, nc, mix, 0)

    slab = ny * weights.depth
    others = {}

    def place_of(q):
        return span(lax.rem(links.z - q + nz, nz), slab)

    def project(q):
        weights.need(2, q)
        at = place_of(q)
        value = lax.dot_general(
            hidden[...],
            held[2, at, :],
            (((1,), (1,)), ((), ())),
            preferred_element_type=jnp.float32,
        )
        sums[:, at] = value[:line]
        for dc in range(1, nc):
            other[dc - 1, :, at] = value[dc * line : (dc + 1) * line].astype(jnp.bfloat16)
            others[q, dc] = links.copy(
                other.at[dc - 1, :, at],
                other_land.at[dc - 1, :, at],
                other_sem,
                (q, dc - 1),
                links.far(dc=nc - dc),
            )

    parts = []

    def settle(q):
        at = place_of(q)
        value = sums[:, at]
        for dc in range(1, nc):
            others[q, dc].wait_recv()
            value = value + other_land[dc - 1, :, at].astype(jnp.float32)
        sums[:, at] = value
        sums_send[:, at] = value.astype(jnp.bfloat16)
        for dz in range(1, nz):
            parts.append(
                links.copy(
                    sums_send.at[span(lax.rem(links.z + dz, nz), own), at],
                    sums_land.at[dz - 1, :, at],
                    sums_sem,
                    (q, dz - 1),
                    links.far(dz=dz),
                )
            )

    for q in range(nz):
        project(q)
        if q:
            settle(q - 1)
    settle(nz - 1)
    for made in parts:
        made.wait_recv()
    total = sums[mine, :]
    for dz in range(1, nz):
        total = total + sums_land[dz - 1].astype(jnp.float32)
    out[...] = (middle.astype(jnp.float32) + 0.5 * rms_scale(total, post_gain[...])).astype(
        jnp.bfloat16
    )
    for made in links.sent:
        made.wait_send()
    for d, copy in enumerate(copies, 1):
        pl.when(me + d < n)(copy.wait_send)


def shards(
    n,
    nt,
    residual,
    inputs,
    pole_real,
    pole_imaginary,
    step_log,
    input_real,
    entry_map_quadrature,
    output_real,
    output_imaginary,
    added_log_decay,
    out_weight,
    mix_gain,
    gate_weight,
    up_weight,
    down_weight,
    pre_gain,
    post_gain,
):
    rows, channels = inputs.shape
    columns = out_weight.shape[1]
    groups, states = pole_real.shape
    width = input_real.shape[2]
    flat = groups * states
    step_size = jnp.exp(step_log)[:, None]
    log_size = pole_real * step_size
    angle = pole_imaginary * step_size
    cosine = jnp.cos(angle)
    sine = jnp.sin(angle)
    magnitude = jnp.exp(log_size)
    lift_real = jnp.expm1(log_size) * cosine - 2.0 * jnp.sin(0.5 * angle) ** 2
    lift_imaginary = magnitude * sine
    denominator = pole_real * pole_real + pole_imaginary * pole_imaginary
    ratio_real = (lift_real * pole_real + lift_imaginary * pole_imaginary) / denominator
    ratio_imaginary = (lift_imaginary * pole_real - lift_real * pole_imaginary) / denominator
    bar_real = (
        ratio_real[..., None] * input_real - ratio_imaginary[..., None] * entry_map_quadrature
    )
    bar_imaginary = (
        ratio_real[..., None] * entry_map_quadrature + ratio_imaginary[..., None] * input_real
    )
    pack = LANES // width
    packs = groups // pack
    same = jnp.eye(pack, dtype=jnp.float32)

    def entry(bar):
        bar = bar.reshape(packs, pack, states, width).transpose(0, 1, 3, 2)
        return (bar[:, :, :, None, :] * same[None, :, None, :, None]).reshape(
            packs, pack * width, pack * states
        )

    def read(weight):
        weight = weight.reshape(packs, pack, width, states).transpose(0, 1, 3, 2)
        return (weight[:, :, :, None, :] * same[None, :, None, :, None]).reshape(
            packs, pack * states, pack * width
        )

    def mixed_rows(values):
        return values.reshape(CHUNKS, rows // CHUNKS, -1).transpose(1, 0, 2).reshape(rows, -1)

    spread = jnp.repeat(mixed_rows(jnp.exp(added_log_decay)), states, axis=1)
    vmem = pl.BlockSpec(memory_space=pltpu.VMEM)
    place = jnp.arange(rows)
    order = jax.nn.one_hot(
        place % (rows // CHUNKS) * CHUNKS + place // (rows // CHUNKS), rows, dtype=jnp.bfloat16
    )
    nz = math.gcd(n, nt)
    ny, nx = n // nz, nt // CORES
    own = rows // nt
    line = nz * own
    depth, units = gate_weight.shape
    piece = -(-units // (LANES * nz)) * LANES
    bf, f32 = jnp.bfloat16, jnp.float32
    return pl.pallas_call(
        functools.partial(layer_kernel, n, nt, nz),
        out_shape=jax.ShapeDtypeStruct((own, columns), bf),
        in_specs=[vmem] * 14 + [pl.BlockSpec(memory_space=pl.ANY)] * 3,
        out_specs=vmem,
        scratch_shapes=[
            pltpu.VMEM((rows, flat), f32),
            pltpu.VMEM((rows, flat), f32),
            pltpu.VMEM((4, CHUNKS, flat), f32),
            pltpu.VMEM((8, flat // 2), f32),
            pltpu.VMEM((n, 8, flat // 2), f32),
            pltpu.VMEM((2, CHUNKS, flat), f32),
            pltpu.VMEM((rows, channels), bf),
            pltpu.VMEM((rows, columns), bf),
            pltpu.VMEM((CORES - 1, nx, own, columns), bf),
            pltpu.VMEM((nx - 1, own, columns), bf),
            pltpu.VMEM((nx - 1, own, columns), bf),
            pltpu.VMEM((3, n * depth, nx * piece), bf),
            pltpu.VMEM((CORES * line, columns), bf),
            pltpu.VMEM((CORES * line, nx * piece), bf),
            pltpu.VMEM((CORES - 1, line, columns), bf),
            pltpu.VMEM((CORES - 1, line, columns), bf),
            pltpu.VMEM((line, columns), f32),
            pltpu.VMEM((line, columns), bf),
            pltpu.VMEM((nz - 1, own, columns), bf),
            pltpu.SemaphoreType.DMA((n - 1,)),
            pltpu.SemaphoreType.DMA((n - 1,)),
            pltpu.SemaphoreType.DMA((3,)),
            pltpu.SemaphoreType.DMA((2, 3, nz - 1)),
            pltpu.SemaphoreType.DMA((2, 3, nz, nx - 1)),
            pltpu.SemaphoreType.DMA((2, 3, nz, ny - 1)),
            pltpu.SemaphoreType.DMA((2, 3, nz, nx - 1, ny - 1)),
            pltpu.SemaphoreType.DMA((2, CORES - 1, nx)),
            pltpu.SemaphoreType.DMA((2, nx - 1)),
            pltpu.SemaphoreType.DMA((2, nz - 1)),
            pltpu.SemaphoreType.DMA((2, nz, CORES - 1)),
            pltpu.SemaphoreType.DMA((2, nz, CORES - 1)),
            pltpu.SemaphoreType.DMA((2, nz, nz - 1)),
        ],
        compiler_params=pltpu.CompilerParams(
            collective_id=0, has_side_effects=True, vmem_limit_bytes=60 * 1024 * 1024
        ),
    )(
        mixed_rows(inputs),
        spread,
        (magnitude * cosine).reshape(1, flat),
        (magnitude * sine).reshape(1, flat),
        entry(bar_real),
        entry(bar_imaginary),
        read(output_real),
        read(-output_imaginary),
        order,
        residual,
        out_weight,
        mix_gain.reshape(1, columns),
        pre_gain.reshape(1, columns),
        post_gain.reshape(1, columns),
        gate_weight,
        up_weight,
        down_weight,
    )


def solution(mesh):
    return jax.shard_map(
        functools.partial(shards, mesh.shape["sp"], mesh.shape["tp"]),
        mesh=mesh,
        in_specs=(
            P(("sp", "tp"), None),
            P("sp", "tp"),
            P("tp", None),
            P("tp", None),
            P("tp"),
            P("tp", None, None),
            P("tp", None, None),
            P("tp", None, None),
            P("tp", None, None),
            P("sp", "tp"),
            P("tp", None),
            P(),
            P("sp", "tp"),
            P("sp", "tp"),
            P("sp", "tp"),
            P(),
            P(),
        ),
        out_specs=P(("sp", "tp"), None),
        check_vma=False,
    )
```

time: 324 us -> 186 us (0.57)
  waiting for transfers between devices: 213 us -> 0 us
  Pallas kernels: 62.1 us -> 163 us
  between operations: 13.4 us -> 0.21 us
  matrix products: 10.4 us -> 0 us
  local copies, waits for them, and re-layouts: 22.8 us -> 15.3 us
  other arithmetic: 2.27 us -> 7.27 us
    all_gather x3 -> x0, waiting for transfers between devices: 210 us -> none  [the longest x1 87.9 us: shards(): lax.all_gather(down_weight, 'sp', axis=0, tiled=True)]
    pallas_call x2 -> x1, Pallas kernels: 62.1 us -> 163 us  [shards(): pl.pallas_call(functools.partial(layer_kernel, n, nt, nz), out_shape=jax....]
    dot_general x2 -> x0, matrix products: 10.4 us -> none  [the longest x1 5.54 us: shards(): jnp.dot(mixer_input, gate_full, preferred_element_type=jnp.float32)]
    mul x9, local copies, waits for them, and re-layouts: 9.86 us -> 4.64 us  [read(): weight[:, :, :, None, :] * same[None, :, None, :, None]]
  transfers between devices with their start and end apart: 3 -> 0, of which waited for: 3 -> 0; matrix products, arithmetic and copies ran while one was open for 9% -> 0% of each run, Pallas kernels for 15% -> 0%
where the time goes in v1:
time: 186 us
  Pallas kernels  163 us (88%)
  local copies, waits for them, and re-layouts  15.3 us (8%)
  other arithmetic  7.27 us (4%)
    pallas_call x1, Pallas kernels, shards(): pl.pallas_call(functools.partial(layer_kernel, n, nt, nz), out_shape=jax....  163 us
    mul x9, local copies, waits for them, and re-layouts, read(): weight[:, :, :, None, :] * same[None, :, None, :, None]  4.64 us

profile of v1, /device:TPU:0, one launch (start us, length us, event | category | flops | bytes accessed | tf_op | source)
XLA Modules:
  0.0 185.5 jit_solution(5771289204813806626)
XLA Ops:
  0.0 0.7 exp.10
  0.7 0.9 fusion.1
  1.6 1.1 multiply_add_fusion
  2.7 0.2 mul.192
  3.0 0.5 mul.193
  3.5 0.2 mul.200
  3.7 1.5 mul.201
  5.2 0.1 copy.24
  5.3 0.1 mul.194
  5.4 0.1 mul.195
  5.6 0.0 copy-start
  5.6 2.9 %broadcast_multiply_fusion.2 = (f32[4,128,512]{2,1,0:T(8,128)}, f32[4,128,512]{2,1,0:T(8,128)}) fusion(f32[4,128,512]{2,1,0:T(8,128)} %mul.201, f32[128,512]{1,0:T(8,128)S(1)} %mul.195, f32[4,128,512]{2,1,0:T(8,128)S(1)} %mul.193), kind=kLoop, calls=%fused_computation.2 | loop fusion | flops 524288 | bytes 4456448 | tf_op jit(solution)/shard_map/mul | solution.py:564
  8.5 0.7 reshape.96.cr
  9.2 0.7 reshape.97.ci
  9.8 0.1 mul.205
  10.0 0.1 mul.206
  10.1 0.1 copy.26
  10.2 0.0 copy-done
  10.3 0.1 copy.28
  10.4 0.2 mul.209
  10.6 0.5 mul.210
  11.1 0.0 copy-start.1
  11.1 0.3 copy.29
  11.4 0.6 copy-done.1
  12.0 0.1 copy.25
  12.1 0.2 mul.203
  12.4 1.5 mul.204
  13.8 1.5 copy.27
  15.4 0.0 copy-start.3
  15.4 1.5 broadcast_multiply_fusion
  16.9 0.0 copy-done.3
  16.9 0.1 reshape.93
  17.0 0.1 copy.22
  17.1 0.1 copy.23
  17.2 0.2 broadcast_in_dim.3
  17.4 0.0 copy-start.2
  17.4 2.1 %copy.30.mag = f32[256,2048]{1,0:T(8,128)} copy(f32[256,2048]{0,1:T(8,128)S(1)} %bitcast.45) | data formatting | bytes 4194304 | tf_op jit(solution)/shard_map/reshape | solution.py:577
  19.4 0.0 copy-done.2
  19.5 0.9 copy.32
  20.3 0.8 fusion.order
  21.1 162.8 %shard_map.163 = bf16[64,2048]{1,0:T(8,128)(2,1)} custom-call(bf16[256,512]{1,0:T(8,128)(2,1)} %bitcast.46, f32[256,2048]{1,0:T(8,128)} %copy.30.mag, f32[1,2048]{1,0:T(1,128)} %reshape.96.cr, f32[1,2048]{1,0:T(1,128)} %reshape.97.ci, f32[4,128,512]{2,1,0:T(8,128)} %get-tuple-element.10.er, f32[4,128,512]{2,1,0:T(8,128)} %get-tuple-element.9.ei, ...), custom_call_target="tpu_custom_call" | custom-call | tf_op jit(solution)/shard_map/pallas_call | solution.py:590
  183.9 1.7 copy.34
  (4 shorter events, 0.0 us)
Async XLA Ops:
  5.6 4.7 %copy-start = (f32[32,16,64]{2,1,0:T(8,128)S(1)}, f32[32,16,64]{2,1,0:T(8,128)}, u32[]{:S(2)}) copy-start(f32[32,16,64]{2,1,0:T(8,128)} %param.25) | copy-start | bytes 393220
  11.1 1.0 copy-start.1
  15.4 1.5 copy-start.3
  17.4 2.1 %copy-start.2 = (bf16[256,512]{1,0:T(8,128)(2,1)S(1)}, bf16[256,512]{1,0:T(8,128)(2,1)}, u32[]{:S(2)}) copy-start(bf16[256,512]{1,0:T(8,128)(2,1)} %param.18) | copy-start | bytes 786436

commit v2 on v1

--- a/solution.py
+++ b/solution.py
@@ -31,6 +31,32 @@
 
 def times(ar, ai, br, bi):
     return ar * br - ai * bi, ar * bi + ai * br
+
+
+def flip(index, mask):
+    out, bit = index, 1
+    while bit <= mask:
+        if mask & bit:
+            out = out + bit - 2 * bit * lax.rem(lax.div(index, bit), 2)
+        bit *= 2
+    return out
+
+
+def mirror(place, size):
+    out = 0
+    while size > 1:
+        out, place, size = 2 * out + place % 2, place // 2, size // 2
+    return out
+
+
+def across(a, b):
+    return lax.dot_general(
+        a, b, (((1,), (1,)), ((), ())), preferred_element_type=jnp.float32
+    )
+
+
+def one_hot(where):
+    return jnp.where(where, 1.0, 0.0).astype(jnp.bfloat16)
 
 
 class Links:
@@ -43,11 +69,11 @@
 
     def far(self, dz=0, dy=0, dx=0, dc=0):
         return {
-            "sp": lax.rem(self.z + dz, self.nz) * self.ny + lax.rem(self.y + dy, self.ny),
+            "sp": flip(self.z, dz) * self.ny + lax.rem(self.y + dy, self.ny),
             "tp": lax.rem(self.x + dx, self.nx) * self.nc + lax.rem(self.c + dc, self.nc),
         }
 
-    def copy(self, src, dst, sems, index, device):
+    def copy(self, src, dst, sems, index, device, when=None):
         made = pltpu.make_async_remote_copy(
             src_ref=src,
             dst_ref=dst,
@@ -56,8 +82,12 @@
             device_id=device,
             device_id_type=MESH,
         )
-        made.start()
-        self.sent.append(made)
+        if when is None:
+            made.start()
+            self.sent.append(made.wait_send)
+        else:
+            pl.when(when)(made.start)
+            self.sent.append(lambda: pl.when(when)(made.wait_send))
         return made
 
 
@@ -77,86 +107,140 @@
         )
         self.depth, self.units = sources[0].shape
         self.wide = held.shape[2] // links.nx
+        self.thin = self.units - (links.nz - 1) * self.wide
         self.coming = {}
 
     def piece(self, z, x):
         links = self.links
         nt = links.nx * links.nc
         tp = x * links.nc + links.c
-        which = lax.rem(z + links.nz * nt - tp - 1, links.nz)
-        first = jnp.minimum(which * self.wide, self.units - self.wide)
-        return which, pl.multiple_of(first, LANES)
-
-    def spot(self, j, dz, dy, slot):
+        return lax.rem(z + links.nz * nt - tp - 1, links.nz)
+
+    def last(self, slot):
         links = self.links
-        origin = lax.rem(links.z - dz + links.nz, links.nz) * links.ny + lax.rem(
-            links.y - dy + links.ny, links.ny
-        )
-        return self.held.at[j, span(origin, self.depth), pl.ds(slot * self.wide, self.wide)]
-
-    def cut(self, j, dz):
+        return self.piece(links.z, lax.rem(links.x - slot + links.nx, links.nx)) == links.nz - 1
+
+    def widths(self, last):
+        if self.thin == self.wide:
+            return ((None, self.wide),)
+        return ((jnp.logical_not(last), self.wide), (last, self.thin))
+
+    def spot(self, j, zr, dy, slot, width):
         links = self.links
-        _, first = self.piece(lax.rem(links.z + dz, links.nz), links.x)
-        return self.sources[j].at[:, pl.ds(first, self.wide)]
+        origin = flip(links.z, zr) * links.ny + lax.rem(links.y - dy + links.ny, links.ny)
+        return self.held.at[j, span(origin, self.depth), pl.ds(slot * self.wide, width)]
+
+    def cut(self, j, which, width):
+        first = jnp.minimum(which * self.wide, self.units - width)
+        return self.sources[j].at[:, pl.ds(pl.multiple_of(first, LANES), width)]
 
     def begin(self):
         links = self.links
+        which = self.piece(links.z, links.x)
         self.own = []
         for j in range(len(self.sources)):
-            own = pltpu.make_async_copy(self.cut(j, 0), self.spot(j, 0, 0, 0), self.local.at[j])
-            own.start()
-            self.own.append(own)
-
-    def along_z(self):
+            for when, width in self.widths(which == links.nz - 1):
+                own = pltpu.make_async_copy(
+                    self.cut(j, which, width), self.spot(j, 0, 0, 0, width), self.local.at[j]
+                )
+                if when is None:
+                    own.start()
+                else:
+                    pl.when(when)(own.start)
+                self.own.append((j, when, own.wait))
+
+    def clear(self):
+        if self.thin < self.wide:
+            for slot in range(self.links.nx):
+
+                @pl.when(self.last(slot))
+                def _():
+                    at = pl.ds(slot * self.wide + self.thin, self.wide - self.thin)
+                    self.held[2, :, at] = jnp.zeros(
+                        (self.held.shape[1], self.wide - self.thin), self.held.dtype
+                    )
+
+    def pass_on(self, key, j, source, target, sems, index, device, last):
+        for when, width in self.widths(last):
+            made = self.links.copy(source(width), target(width), sems, index, device, when)
+            self.coming.setdefault(key, []).append(made)
+
+    def along_z(self, j, zr):
         links = self.links
-        for j in range(len(self.sources)):
-            for dz in range(1, links.nz):
-                self.coming["z", j, dz] = links.copy(
-                    self.cut(j, dz), self.spot(j, 0, 0, 0), self.z_sem, (j, dz - 1), links.far(dz=dz)
-                )
+        which = self.piece(flip(links.z, zr), links.x)
+        self.pass_on(
+            ("z", j, zr),
+            j,
+            lambda width: self.cut(j, which, width),
+            lambda width: self.spot(j, 0, 0, 0, width),
+            self.z_sem,
+            (j, zr - 1),
+            links.far(dz=zr),
+            which == links.nz - 1,
+        )
 
     def arrive(self, *key):
+        slot = {"z": 0, "y": 0, "x": key[-1], "d": key[3] if len(key) > 4 else 0}[key[0]]
         made = self.coming.pop(key, None)
         if made is not None:
-            made.wait_recv()
+            for one, (when, _) in zip(made, self.widths(self.last(slot))):
+                if when is None:
+                    one.wait_recv()
+                else:
+                    pl.when(when)(one.wait_recv)
 
     def spread(self, j, zr):
         links = self.links
         if zr == 0:
-            self.own[j].wait()
+            for at, when, wait in self.own:
+                if at == j:
+                    wait() if when is None else pl.when(when)(wait)
         else:
             self.arrive("z", j, zr)
-        here = self.spot(j, zr, 0, 0)
+        last = self.last(0)
         for dx in range(1, links.nx):
-            self.coming["x", j, zr, dx] = links.copy(
-                here, self.spot(j, zr, 0, dx), self.x_sem, (j, zr, dx - 1), links.far(dx=dx)
+            self.pass_on(
+                ("x", j, zr, dx),
+                j,
+                lambda width: self.spot(j, zr, 0, 0, width),
+                lambda width: self.spot(j, zr, 0, dx, width),
+                self.x_sem,
+                (j, zr, dx - 1),
+                links.far(dx=dx),
+                last,
             )
         for dy in range(1, links.ny):
-            self.coming["y", j, zr, dy] = links.copy(
-                here, here, self.y_sem, (j, zr, dy - 1), links.far(dy=dy)
+            self.pass_on(
+                ("y", j, zr, dy),
+                j,
+                lambda width: self.spot(j, zr, 0, 0, width),
+                lambda width: self.spot(j, zr, 0, 0, width),
+                self.y_sem,
+                (j, zr, dy - 1),
+                links.far(dy=dy),
+                last,
             )
 
     def relay(self, j, zr):
         links = self.links
-        if (j + zr) % 2 == 0:
-            for dx in range(1, links.nx):
+        over_y = (j + zr) % 2 == 0
+        for dx in range(1, links.nx):
+            if over_y:
                 self.arrive("x", j, zr, dx)
-                here = self.spot(j, zr, 0, dx)
-                for dy in range(1, links.ny):
-                    self.coming["d", j, zr, dx, dy] = links.copy(
-                        here, here, self.d_sem, (j, zr, dx - 1, dy - 1), links.far(dy=dy)
-                    )
-        else:
             for dy in range(1, links.ny):
-                self.arrive("y", j, zr, dy)
-                for dx in range(1, links.nx):
-                    self.coming["d", j, zr, dx, dy] = links.copy(
-                        self.spot(j, zr, dy, 0),
-                        self.spot(j, zr, dy, dx),
-                        self.d_sem,
-                        (j, zr, dx - 1, dy - 1),
-                        links.far(dx=dx),
-                    )
+                if not over_y:
+                    self.arrive("y", j, zr, dy)
+                slot, shift = (dx, 0) if over_y else (0, dy)
+                self.pass_on(
+                    ("d", j, zr, dx, dy),
+                    j,
+                    lambda width: self.spot(j, zr, shift, slot, width),
+                    lambda width: self.spot(j, zr, shift, dx, width),
+                    self.d_sem,
+                    (j, zr, dx - 1, dy - 1),
+                    links.far(dy=dy) if over_y else links.far(dx=dx),
+                    self.last(slot),
+                )
 
     def need(self, j, zr):
         for key in [key for key in self.coming if key[1:3] == (j, zr)]:
@@ -168,14 +252,10 @@
     nt,
     nz,
     u,
-    mag,
-    cr,
-    ci,
-    er,
-    ei,
-    rr,
-    ri,
-    order,
+    added,
+    lines,
+    entry,
+    read,
     residual,
     weight,
     mix_gain,
@@ -185,6 +265,7 @@
     up_weight,
     down_weight,
     out,
+    mag,
     dr,
     di,
     ends,
@@ -224,7 +305,9 @@
     rows, flat = dr.shape
     own = rows // nt
     steps = rows // CHUNKS
-    packs, width, wide = er.shape
+    states, width = flat // added.shape[1], entry.shape[1]
+    pack = LANES // width
+    packs, wide = added.shape[1] // pack, pack * states
     block = min(BLOCK, flat)
 
     barrier = pltpu.get_barrier_semaphore()
@@ -242,15 +325,46 @@
     )
     weights.begin()
     pl.semaphore_wait(barrier, n - 1 + nt - 1)
-    weights.along_z()
+    for j in range(2):
+        for zr in range(1, nz):
+            weights.along_z(j, zr)
     for j in range(3):
         weights.spread(j, 0)
-
+    weights.clear()
+
+    down = lax.broadcasted_iota(jnp.int32, (rows, rows), 0)
+    over = lax.broadcasted_iota(jnp.int32, (rows, rows), 1)
+    mixing = one_hot(over == lax.rem(down, CHUNKS) * steps + lax.div(down, CHUNKS))
+    order = one_hot(over == lax.rem(down, steps) * CHUNKS + lax.div(down, steps))
+    mixed_u = dot32(mixing, u[...]).astype(jnp.bfloat16)
+    groups = added.shape[1]
+    repeat = one_hot(
+        lax.div(lax.broadcasted_iota(jnp.int32, (groups, flat), 1), states)
+        == lax.broadcasted_iota(jnp.int32, (groups, flat), 0)
+    )
+    rest = jnp.exp(added[...])
+    total = None
+    for _ in range(3):
+        term = rest.astype(jnp.bfloat16)
+        rest = rest - term.astype(jnp.float32)
+        term = dot32(dot32(mixing, term).astype(jnp.bfloat16), repeat)
+        total = term if total is None else total + term
+    mag[...] = total
+    same = lax.div(
+        lax.broadcasted_iota(jnp.int32, (LANES, wide), 0), width
+    ) == lax.div(lax.broadcasted_iota(jnp.int32, (LANES, wide), 1), states)
+
+    def blocks(rows_of_channels):
+        return jnp.where(same, jnp.concatenate([rows_of_channels] * pack, axis=0), 0.0)
+
+    cr, ci = lines.at[0:1], lines.at[1:2]
     for p in range(packs):
-        piece = u[:, p * width : (p + 1) * width]
-        for e, dst in ((er, dr), (ei, di)):
-            high, low = split(e[p])
-            dst[:, p * wide : (p + 1) * wide] = dot32(piece, high) + dot32(piece, low)
+        at = pl.ds(p * wide, wide)
+        piece = mixed_u[:, p * LANES : (p + 1) * LANES]
+        ratio = times(lines[2:3, at], lines[3:4, at], entry[0, :, at], entry[1, :, at])
+        for bar, dst in zip(ratio, (dr, di)):
+            high, low = split(blocks(bar))
+            dst[:, at] = dot32(piece, high) + dot32(piece, low)
 
     for b in range(0, flat, block):
         at = pl.ds(b, block)
@@ -294,11 +408,7 @@
         pl.when(me + d < n)(copy.start)
         copies.append(copy)
 
-    for j in range(3):
-        weights.relay(j, 0)
-    for zr in range(1, nz):
-        weights.spread(0, zr)
-
+    weights.relay(0, 0)
     for d, copy in enumerate(copies, 1):
         pl.when(me >= d)(copy.wait_recv)
 
@@ -337,14 +447,15 @@
 
     for p in range(packs):
         total = None
-        for state, read in ((dr, rr), (di, ri)):
-            high, low = split(state[:, p * wide : (p + 1) * wide])
-            top, rest = split(read[p])
-            term = dot32(high, top) + dot32(high, rest) + dot32(low, top)
+        at = pl.ds(p * wide, wide)
+        for state, part_read in ((dr, read[0, :, at]), (di, -read[1, :, at])):
+            high, low = split(state[:, at])
+            top, rest = split(blocks(part_read))
+            term = across(high, top) + across(high, rest) + across(low, top)
             total = term if total is None else total + term
-        active[:, p * width : (p + 1) * width] = jax.nn.gelu(total).astype(jnp.bfloat16)
-
-    active[...] = dot32(order[...], active[...]).astype(jnp.bfloat16)
+        active[:, p * LANES : (p + 1) * LANES] = jax.nn.gelu(total).astype(jnp.bfloat16)
+
+    active[...] = dot32(order, active[...]).astype(jnp.bfloat16)
     columns = weight.shape[1]
     for b in range(0, columns, BLOCK):
         at = pl.ds(b, BLOCK)
@@ -365,8 +476,10 @@
                     links.far(dc=dc),
                 )
             )
+    weights.relay(1, 0)
+    weights.relay(2, 0)
     for zr in range(1, nz):
-        weights.relay(0, zr)
+        weights.spread(0, zr)
     for made in pairs:
         made.wait_recv()
 
@@ -390,40 +503,50 @@
         jnp.bfloat16
     )
     line = nz * own
-    mine = span(links.z, own)
-    rows_all[mine, :] = rms_scale(middle.astype(jnp.float32), pre_gain[...]).astype(jnp.bfloat16)
-    along = []
-    for dz in range(1, nz):
-        along.append(
-            links.copy(rows_all.at[mine], rows_all.at[mine], row_sem, (dz - 1,), links.far(dz=dz))
-        )
+    bits = [1 << k for k in range(nz.bit_length() - 1)]
+    rows_all[:own] = rms_scale(middle.astype(jnp.float32), pre_gain[...]).astype(jnp.bfloat16)
+    along = {}
     to_pair = []
 
-    def hand_over(zr):
-        index = lax.rem(links.z - zr + nz, nz)
+    def row_block(zr, dc=0):
+        return pl.ds(dc * line + mirror(zr, nz) * own, own)
+
+    def hand_on(zr):
+        if zr:
+            along[zr].wait_recv()
+        for bit in reversed(bits):
+            if zr == 0 or bit < (zr & -zr):
+                along[zr ^ bit] = links.copy(
+                    rows_all.at[row_block(zr)],
+                    rows_all.at[row_block(zr ^ bit)],
+                    row_sem,
+                    ((zr ^ bit) - 1,),
+                    links.far(dz=bit),
+                )
         for dc in range(1, nc):
             to_pair.append(
                 links.copy(
-                    rows_all.at[span(index, own)],
-                    rows_all.at[span(dc * nz + index, own)],
+                    rows_all.at[row_block(zr)],
+                    rows_all.at[row_block(zr, dc)],
                     row_pair_sem,
                     (zr, dc - 1),
                     links.far(dc=dc),
                 )
             )
 
-    hand_over(0)
+    hand_on(0)
+    for zr in range(1, nz):
+        weights.along_z(2, zr)
+    for zr in range(1, nz):
+        weights.relay(0, zr)
     for zr in range(1, nz):
         weights.spread(1, zr)
+    for zr in sorted(range(1, nz), key=lambda zr: -(zr & -zr)):
+        hand_on(zr)
     for zr in range(1, nz):
         weights.relay(1, zr)
     for zr in range(1, nz):
         weights.spread(2, zr)
-    for zr in range(1, nz):
-        along[zr - 1].wait_recv()
-        hand_over(zr)
-    for zr in range(1, nz):
-        weights.relay(2, zr)
     for made in to_pair:
         made.wait_recv()
     for j in range(2):
@@ -432,35 +555,33 @@
 
     valid = []
     for slot in range(nx):
-        which, begin = weights.piece(links.z, lax.rem(links.x - slot + nx, nx))
         at = lax.broadcasted_iota(jnp.int32, (1, weights.wide), 1)
-        valid.append(jnp.where(begin + at >= which * weights.wide, 1.0, 0.0))
+        limit = jnp.where(weights.last(slot), weights.thin, weights.wide)
+        valid.append(jnp.where(at < limit, 1.0, 0.0))
     valid = jnp.concatenate(valid, axis=1)
 
     def mix(b, carry):
         at = span(b, line)
         gate = dot32(rows_all[at, :], held[0])
         up = dot32(rows_all[at, :], held[1])
-        hidden[at, :] = (jax.nn.silu(gate) * up * valid).astype(jnp.bfloat16)
+        hidden[at, :] = jnp.where(valid > 0.0, jax.nn.silu(gate) * up, 0.0).astype(jnp.bfloat16)
         return carry
 
     lax.fori_loop(0, nc, mix, 0)
+    for zr in range(1, nz):
+        weights.relay(2, zr)
 
     slab = ny * weights.depth
     others = {}
+    parts = {}
 
     def place_of(q):
-        return span(lax.rem(links.z - q + nz, nz), slab)
+        return span(flip(links.z, q), slab)
 
     def project(q):
         weights.need(2, q)
         at = place_of(q)
-        value = lax.dot_general(
-            hidden[...],
-            held[2, at, :],
-            (((1,), (1,)), ((), ())),
-            preferred_element_type=jnp.float32,
-        )
+        value = across(hidden[...], held[2, at, :])
         sums[:, at] = value[:line]
         for dc in range(1, nc):
             other[dc - 1, :, at] = value[dc * line : (dc + 1) * line].astype(jnp.bfloat16)
@@ -472,7 +593,29 @@
                 links.far(dc=nc - dc),
             )
 
-    parts = []
+    def give(q, level, value):
+        if level == len(bits):
+            sums[:own, place_of(q)] = value
+            return
+        at = place_of(q)
+        count = value.shape[0] // 2
+        half_rows = pl.ds(count, count)
+        sums[:count, at] = value[:count]
+        sums_send[half_rows, at] = value[count:].astype(jnp.bfloat16)
+        parts[q ^ bits[level], level] = links.copy(
+            sums_send.at[half_rows, at],
+            sums_land.at[half_rows, at],
+            sums_sem,
+            (q ^ bits[level], level),
+            links.far(dz=bits[level]),
+        )
+
+    def take(q, level):
+        at = place_of(q)
+        count = line >> (level + 1)
+        parts[q, level].wait_recv()
+        land = sums_land[pl.ds(count, count), at].astype(jnp.float32)
+        give(q, level + 1, sums[:count, at] + land)
 
     def settle(q):
         at = place_of(q)
@@ -480,34 +623,28 @@
         for dc in range(1, nc):
             others[q, dc].wait_recv()
             value = value + other_land[dc - 1, :, at].astype(jnp.float32)
-        sums[:, at] = value
-        sums_send[:, at] = value.astype(jnp.bfloat16)
-        for dz in range(1, nz):
-            parts.append(
-                links.copy(
-                    sums_send.at[span(lax.rem(links.z + dz, nz), own), at],
-                    sums_land.at[dz - 1, :, at],
-                    sums_sem,
-                    (q, dz - 1),
-                    links.far(dz=dz),
-                )
-            )
-
+        give(q, 0, value)
+
+    taken = 0
     for q in range(nz):
         project(q)
-        if q:
-            settle(q - 1)
-    settle(nz - 1)
-    for made in parts:
-        made.wait_recv()
-    total = sums[mine, :]
-    for dz in range(1, nz):
-        total = total + sums_land[dz - 1].astype(jnp.float32)
+        if q % 2 or q == nz - 1:
+            for done in range(q - q % 2, q + 1):
+                settle(done)
+            while bits and taken < q - 1:
+                take(taken, 0)
+                taken += 1
+    for q in range(taken if bits else nz, nz):
+        take(q, 0)
+    for level in range(1, len(bits)):
+        for q in range(nz):
+            take(q, level)
+    total = sums[:own, :]
     out[...] = (middle.astype(jnp.float32) + 0.5 * rms_scale(total, post_gain[...])).astype(
         jnp.bfloat16
     )
-    for made in links.sent:
-        made.wait_send()
+    for wait in links.sent:
+        wait()
     for d, copy in enumerate(copies, 1):
         pl.when(me + d < n)(copy.wait_send)
 
@@ -549,38 +686,14 @@
     denominator = pole_real * pole_real + pole_imaginary * pole_imaginary
     ratio_real = (lift_real * pole_real + lift_imaginary * pole_imaginary) / denominator
     ratio_imaginary = (lift_imaginary * pole_real - lift_real * pole_imaginary) / denominator
-    bar_real = (
-        ratio_real[..., None] * input_real - ratio_imaginary[..., None] * entry_map_quadrature
-    )
-    bar_imaginary = (
-        ratio_real[..., None] * entry_map_quadrature + ratio_imaginary[..., None] * input_real
-    )
-    pack = LANES // width
-    packs = groups // pack
-    same = jnp.eye(pack, dtype=jnp.float32)
-
-    def entry(bar):
-        bar = bar.reshape(packs, pack, states, width).transpose(0, 1, 3, 2)
-        return (bar[:, :, :, None, :] * same[None, :, None, :, None]).reshape(
-            packs, pack * width, pack * states
-        )
-
-    def read(weight):
-        weight = weight.reshape(packs, pack, width, states).transpose(0, 1, 3, 2)
-        return (weight[:, :, :, None, :] * same[None, :, None, :, None]).reshape(
-            packs, pack * states, pack * width
-        )
-
-    def mixed_rows(values):
-        return values.reshape(CHUNKS, rows // CHUNKS, -1).transpose(1, 0, 2).reshape(rows, -1)
-
-    spread = jnp.repeat(mixed_rows(jnp.exp(added_log_decay)), states, axis=1)
+    lines = jnp.stack(
+        (magnitude * cosine, magnitude * sine, ratio_real, ratio_imaginary)
+    ).reshape(4, flat)
+    entry = jnp.stack((input_real, entry_map_quadrature)).transpose(0, 3, 1, 2)
+    read = jnp.stack((output_real, output_imaginary)).transpose(0, 2, 1, 3)
     vmem = pl.BlockSpec(memory_space=pltpu.VMEM)
-    place = jnp.arange(rows)
-    order = jax.nn.one_hot(
-        place % (rows // CHUNKS) * CHUNKS + place // (rows // CHUNKS), rows, dtype=jnp.bfloat16
-    )
     nz = math.gcd(n, nt)
+    nz = nz & -nz
     ny, nx = n // nz, nt // CORES
     own = rows // nt
     line = nz * own
@@ -590,9 +703,10 @@
     return pl.pallas_call(
         functools.partial(layer_kernel, n, nt, nz),
         out_shape=jax.ShapeDtypeStruct((own, columns), bf),
-        in_specs=[vmem] * 14 + [pl.BlockSpec(memory_space=pl.ANY)] * 3,
+        in_specs=[vmem] * 10 + [pl.BlockSpec(memory_space=pl.ANY)] * 3,
         out_specs=vmem,
         scratch_shapes=[
+            pltpu.VMEM((rows, flat), f32),
             pltpu.VMEM((rows, flat), f32),
             pltpu.VMEM((rows, flat), f32),
             pltpu.VMEM((4, CHUNKS, flat), f32),
@@ -611,7 +725,7 @@
             pltpu.VMEM((CORES - 1, line, columns), bf),
             pltpu.VMEM((line, columns), f32),
             pltpu.VMEM((line, columns), bf),
-            pltpu.VMEM((nz - 1, own, columns), bf),
+            pltpu.VMEM((line, columns), bf),
             pltpu.SemaphoreType.DMA((n - 1,)),
             pltpu.SemaphoreType.DMA((n - 1,)),
             pltpu.SemaphoreType.DMA((3,)),
@@ -624,21 +738,17 @@
             pltpu.SemaphoreType.DMA((2, nz - 1)),
             pltpu.SemaphoreType.DMA((2, nz, CORES - 1)),
             pltpu.SemaphoreType.DMA((2, nz, CORES - 1)),
-            pltpu.SemaphoreType.DMA((2, nz, nz - 1)),
+            pltpu.SemaphoreType.DMA((2, nz, nz.bit_length())),
         ],
         compiler_params=pltpu.CompilerParams(
             collective_id=0, has_side_effects=True, vmem_limit_bytes=60 * 1024 * 1024
         ),
     )(
-        mixed_rows(inputs),
-        spread,
-        (magnitude * cosine).reshape(1, flat),
-        (magnitude * sine).reshape(1, flat),
-        entry(bar_real),
-        entry(bar_imaginary),
-        read(output_real),
-        read(-output_imaginary),
-        order,
+        inputs,
+        added_log_decay,
+        lines,
+        entry.reshape(2, width, flat),
+        read.reshape(2, width, flat),
         residual,
         out_weight,
         mix_gain.reshape(1, columns),

time: 186 us -> 157 us (0.84)
  the two profiles are of different devices: /device:TPU:0 before, /device:TPU:10 now
where the time goes in v2:
time: 157 us
  Pallas kernels  148 us (94%)
  local copies, waits for them, and re-layouts  5.54 us (4%)
  other arithmetic  2.69 us (2%)
    pallas_call x1, Pallas kernels, shards(): pl.pallas_call(functools.partial(layer_kernel, n, nt, nz), out_shape=jax....  148 us

profile of v2, /device:TPU:10, one launch (start us, length us, event | category | flops | bytes accessed | tf_op | source)
XLA Modules:
  0.0 156.7 jit_solution(17461012265650518520)
XLA Ops:
  0.0 0.0 copy-start.1
  0.0 0.0 copy-start
  0.0 0.7 exp.6
  0.7 1.0 fusion.1
  1.7 0.1 stack.33
  1.8 0.1 stack.34
  1.8 0.1 stack.35
  1.9 0.1 stack.36
  2.0 0.6 pad_maximum_fusion.lines
  2.6 1.1 maximum_bitcast_fusion
  3.7 0.2 copy.18
  3.9 0.0 copy-start.2
  3.9 0.9 reshape.25.entry
  4.8 0.0 copy-done.1
  4.8 0.0 copy-done
  4.8 0.2 copy.19
  5.0 0.9 reshape.26.read
  5.9 0.0 copy-done.2
  5.9 0.7 copy.20.added
  6.6 148.4 %shard_map.163 = bf16[64,2048]{1,0:T(8,128)(2,1)} custom-call(bf16[256,512]{1,0:T(8,128)(2,1)} %u.1, f32[256,32]{1,0:T(8,128)} %copy.20.added, f32[4,2048]{1,0:T(4,128)} %pad_maximum_fusion.lines, f32[2,16,2048]{2,1,0:T(8,128)} %reshape.25.entry, f32[2,16,2048]{2,1,0:T(8,128)} %reshape.26.read, bf16[64,2048]{1,0:T(8,128)(2,1)} %residual.1, ...), custom_call_target="tpu_custom_call" | custom-call | tf_op jit(solution)/shard_map/pallas_call | solution.py:703
  155.0 1.7 %copy.22 = bf16[64,2048]{1,0:T(8,128)(2,1)} copy(bf16[64,2048]{1,0:T(8,128)(2,1)} %shard_map.163) | data formatting | bytes 524288
  (1 shorter events, 0.0 us)
Async XLA Ops:
  0.0 4.8 %copy-start.1 = (f32[32,16,64]{2,1,0:T(8,128)S(1)}, f32[32,16,64]{2,1,0:T(8,128)}, u32[]{:S(2)}) copy-start(f32[32,16,64]{2,1,0:T(8,128)} %param.24) | copy-start | bytes 393220
  0.0 4.8 %copy-start = (f32[32,16,64]{2,1,0:T(8,128)S(1)}, f32[32,16,64]{2,1,0:T(8,128)}, u32[]{:S(2)}) copy-start(f32[32,16,64]{2,1,0:T(8,128)} %param.25) | copy-start | bytes 393220
  3.9 2.0 %copy-start.2 = (f32[256,32]{0,1:T(8,128)S(1)}, f32[256,32]{0,1:T(8,128)}, u32[]{:S(2)}) copy-start(f32[256,32]{0,1:T(8,128)} %param.26) | copy-start | bytes 98308

commit v3 on v2

--- a/solution.py
+++ b/solution.py
@@ -96,8 +96,8 @@
 
 
 class Weights:
-    def __init__(self, links, sources, held, local, z_sem, x_sem, y_sem, d_sem):
-        self.links, self.sources, self.held = links, sources, held
+    def __init__(self, links, sources, staged, held, local, z_sem, x_sem, y_sem, d_sem):
+        self.links, self.sources, self.staged, self.held = links, sources, staged, held
         self.local, self.z_sem, self.x_sem, self.y_sem, self.d_sem = (
             local,
             z_sem,
@@ -130,18 +130,25 @@
         origin = flip(links.z, zr) * links.ny + lax.rem(links.y - dy + links.ny, links.ny)
         return self.held.at[j, span(origin, self.depth), pl.ds(slot * self.wide, width)]
 
-    def cut(self, j, which, width):
+    def cut(self, source, which, width):
         first = jnp.minimum(which * self.wide, self.units - width)
-        return self.sources[j].at[:, pl.ds(pl.multiple_of(first, LANES), width)]
+        return source.at[:, pl.ds(pl.multiple_of(first, LANES), width)]
 
     def begin(self):
         links = self.links
         which = self.piece(links.z, links.x)
         self.own = []
+        self.whole = [
+            pltpu.make_async_copy(source, self.staged.at[j], self.local.at[1, j])
+            for j, source in enumerate(self.sources)
+        ]
         for j in range(len(self.sources)):
+            self.whole[j].start()
             for when, width in self.widths(which == links.nz - 1):
                 own = pltpu.make_async_copy(
-                    self.cut(j, which, width), self.spot(j, 0, 0, 0, width), self.local.at[j]
+                    self.cut(self.sources[j], which, width),
+                    self.spot(j, 0, 0, 0, width),
+                    self.local.at[0, j],
                 )
                 if when is None:
                     own.start()
@@ -168,10 +175,12 @@
     def along_z(self, j, zr):
         links = self.links
         which = self.piece(flip(links.z, zr), links.x)
+        if zr == 1:
+            self.whole[j].wait()
         self.pass_on(
             ("z", j, zr),
             j,
-            lambda width: self.cut(j, which, width),
+            lambda width: self.cut(self.staged.at[j], which, width),
             lambda width: self.spot(j, 0, 0, 0, width),
             self.z_sem,
             (j, zr - 1),
@@ -277,6 +286,7 @@
     pair_land,
     half,
     half_land,
+    staged,
     held,
     rows_all,
     hidden,
@@ -321,15 +331,18 @@
             barrier, inc=1, device_id={"tp": lax.rem(place + d, nt)}, device_id_type=MESH
         )
     weights = Weights(
-        links, (gate_weight, up_weight, down_weight), held, local_sem, z_sem, x_sem, y_sem, d_sem
+        links, (gate_weight, up_weight, down_weight), staged, held, local_sem, z_sem, x_sem, y_sem, d_sem
     )
     weights.begin()
     pl.semaphore_wait(barrier, n - 1 + nt - 1)
-    for j in range(2):
-        for zr in range(1, nz):
-            weights.along_z(j, zr)
-    for j in range(3):
-        weights.spread(j, 0)
+    near, far = range(1, min(2, nz)), range(2, nz)
+
+    def each(step, j, reach):
+        for zr in reach:
+            step(j, zr)
+
+    each(weights.along_z, 0, near)
+    weights.spread(0, 0)
     weights.clear()
 
     down = lax.broadcasted_iota(jnp.int32, (rows, rows), 0)
@@ -408,9 +421,11 @@
         pl.when(me + d < n)(copy.start)
         copies.append(copy)
 
-    weights.relay(0, 0)
     for d, copy in enumerate(copies, 1):
         pl.when(me >= d)(copy.wait_recv)
+    weights.spread(1, 0)
+    weights.spread(2, 0)
+    weights.relay(0, 0)
 
     sr = jnp.zeros((1, flat), jnp.float32)
     si = sr
@@ -461,6 +476,9 @@
         at = pl.ds(b, BLOCK)
         part[:, at] = dot32(active[...], weight[:, at]).astype(jnp.bfloat16)
 
+    each(weights.along_z, 0, far)
+    each(weights.along_z, 1, near)
+
     def rows_of(x, c):
         return span(x * nc + c, own)
 
@@ -476,10 +494,6 @@
                     links.far(dc=dc),
                 )
             )
-    weights.relay(1, 0)
-    weights.relay(2, 0)
-    for zr in range(1, nz):
-        weights.spread(0, zr)
     for made in pairs:
         made.wait_recv()
 
@@ -495,6 +509,9 @@
         halves.append(
             links.copy(half.at[dx - 1], half_land.at[dx - 1], half_sem, (dx - 1,), links.far(dx=dx))
         )
+    each(weights.spread, 0, near)
+    weights.relay(1, 0)
+    weights.relay(2, 0)
     mixed = chip_sum(links.x)
     for dx, made in enumerate(halves):
         made.wait_recv()
@@ -535,18 +552,29 @@
             )
 
     hand_on(0)
-    for zr in range(1, nz):
-        weights.along_z(2, zr)
-    for zr in range(1, nz):
-        weights.relay(0, zr)
-    for zr in range(1, nz):
-        weights.spread(1, zr)
+    each(weights.spread, 0, far)
+    each(weights.relay, 0, near)
+    meanwhile = [
+        [
+            (weights.along_z, 1, far),
+            (weights.relay, 0, far),
+            (weights.spread, 1, near),
+            (weights.relay, 1, near),
+        ],
+        [],
+        [(weights.along_z, 2, range(1, nz))],
+    ]
     for zr in sorted(range(1, nz), key=lambda zr: -(zr & -zr)):
         hand_on(zr)
-    for zr in range(1, nz):
-        weights.relay(1, zr)
-    for zr in range(1, nz):
-        weights.spread(2, zr)
+        for item in meanwhile.pop(0) if meanwhile else ():
+            each(*item)
+    for items in meanwhile:
+        for item in items:
+            each(*item)
+    each(weights.spread, 1, far)
+    each(weights.relay, 1, far)
+    each(weights.spread, 2, near)
+    each(weights.relay, 2, near)
     for made in to_pair:
         made.wait_recv()
     for j in range(2):
@@ -568,8 +596,7 @@
         return carry
 
     lax.fori_loop(0, nc, mix, 0)
-    for zr in range(1, nz):
-        weights.relay(2, zr)
+    each(weights.spread, 2, far)
 
     slab = ny * weights.depth
     others = {}
@@ -625,16 +652,20 @@
             value = value + other_land[dc - 1, :, at].astype(jnp.float32)
         give(q, 0, value)
 
-    taken = 0
-    for q in range(nz):
+    ready = min(2, nz)
+    for q in range(ready):
         project(q)
-        if q % 2 or q == nz - 1:
-            for done in range(q - q % 2, q + 1):
-                settle(done)
-            while bits and taken < q - 1:
-                take(taken, 0)
-                taken += 1
-    for q in range(taken if bits else nz, nz):
+    for q in range(ready):
+        settle(q)
+    each(weights.relay, 2, far)
+    if bits:
+        for q in range(ready):
+            take(q, 0)
+    for q in range(ready, nz):
+        project(q)
+    for q in range(ready, nz):
+        settle(q)
+    for q in range(ready, nz):
         take(q, 0)
     for level in range(1, len(bits)):
         for q in range(nz):
@@ -718,6 +749,7 @@
             pltpu.VMEM((CORES - 1, nx, own, columns), bf),
             pltpu.VMEM((nx - 1, own, columns), bf),
             pltpu.VMEM((nx - 1, own, columns), bf),
+            pltpu.VMEM((3, depth, units), bf),
             pltpu.VMEM((3, n * depth, nx * piece), bf),
             pltpu.VMEM((CORES * line, columns), bf),
             pltpu.VMEM((CORES * line, nx * piece), bf),
@@ -728,7 +760,7 @@
             pltpu.VMEM((line, columns), bf),
             pltpu.SemaphoreType.DMA((n - 1,)),
             pltpu.SemaphoreType.DMA((n - 1,)),
-            pltpu.SemaphoreType.DMA((3,)),
+            pltpu.SemaphoreType.DMA((2, 3)),
             pltpu.SemaphoreType.DMA((2, 3, nz - 1)),
             pltpu.SemaphoreType.DMA((2, 3, nz, nx - 1)),
             pltpu.SemaphoreType.DMA((2, 3, nz, ny - 1)),

time: 157 us -> 131 us (0.83)
  the two profiles are of different devices: /device:TPU:10 before, /device:TPU:0 now
where the time goes in v3:
time: 131 us
  Pallas kernels  123 us (94%)
  local copies, waits for them, and re-layouts  5.54 us (4%)
  other arithmetic  2.69 us (2%)
    pallas_call x1, Pallas kernels, shards(): pl.pallas_call(functools.partial(layer_kernel, n, nt, nz), out_shape=jax....  123 us

profile of v3, /device:TPU:0, one launch (start us, length us, event | category | flops | bytes accessed | tf_op | source)
XLA Modules:
  0.0 130.9 jit_solution(11690926576777160578)
XLA Ops:
  0.0 0.0 copy-start.1
  0.0 0.0 copy-start
  0.0 0.7 exp.6
  0.7 1.0 fusion.1
  1.7 0.1 stack.33
  1.8 0.1 stack.34
  1.8 0.1 stack.35
  1.9 0.1 stack.36
  2.0 0.6 pad_maximum_fusion.lines
  2.6 1.1 maximum_bitcast_fusion
  3.7 0.2 copy.18
  3.9 0.0 copy-start.2
  3.9 0.9 reshape.25.entry
  4.8 0.0 copy-done.1
  4.8 0.0 copy-done
  4.8 0.2 copy.19
  5.0 0.9 reshape.26.read
  5.9 0.0 copy-done.2
  5.9 0.7 copy.20.added
  6.6 122.6 %shard_map.163 = bf16[64,2048]{1,0:T(8,128)(2,1)} custom-call(bf16[256,512]{1,0:T(8,128)(2,1)} %u.1, f32[256,32]{1,0:T(8,128)} %copy.20.added, f32[4,2048]{1,0:T(4,128)} %pad_maximum_fusion.lines, f32[2,16,2048]{2,1,0:T(8,128)} %reshape.25.entry, f32[2,16,2048]{2,1,0:T(8,128)} %reshape.26.read, bf16[64,2048]{1,0:T(8,128)(2,1)} %residual.1, ...), custom_call_target="tpu_custom_call" | custom-call | tf_op jit(solution)/shard_map/pallas_call | solution.py:734
  129.2 1.7 %copy.22 = bf16[64,2048]{1,0:T(8,128)(2,1)} copy(bf16[64,2048]{1,0:T(8,128)(2,1)} %shard_map.163) | data formatting | bytes 524288
  (1 shorter events, 0.0 us)
Async XLA Ops:
  0.0 4.8 %copy-start.1 = (f32[32,16,64]{2,1,0:T(8,128)S(1)}, f32[32,16,64]{2,1,0:T(8,128)}, u32[]{:S(2)}) copy-start(f32[32,16,64]{2,1,0:T(8,128)} %param.24) | copy-start | bytes 393220
  0.0 4.8 %copy-start = (f32[32,16,64]{2,1,0:T(8,128)S(1)}, f32[32,16,64]{2,1,0:T(8,128)}, u32[]{:S(2)}) copy-start(f32[32,16,64]{2,1,0:T(8,128)} %param.25) | copy-start | bytes 393220
  3.9 2.0 %copy-start.2 = (f32[256,32]{0,1:T(8,128)S(1)}, f32[256,32]{0,1:T(8,128)}, u32[]{:S(2)}) copy-start(f32[256,32]{0,1:T(8,128)} %param.26) | copy-start | bytes 98308

commit v4 on v3

--- a/solution.py
+++ b/solution.py
@@ -478,6 +478,7 @@
 
     each(weights.along_z, 0, far)
     each(weights.along_z, 1, near)
+    each(weights.along_z, 2, near)
 
     def rows_of(x, c):
         return span(x * nc + c, own)
@@ -552,26 +553,25 @@
             )
 
     hand_on(0)
+    each(weights.along_z, 1, far)
     each(weights.spread, 0, far)
     each(weights.relay, 0, near)
     meanwhile = [
         [
-            (weights.along_z, 1, far),
             (weights.relay, 0, far),
             (weights.spread, 1, near),
             (weights.relay, 1, near),
-        ],
-        [],
-        [(weights.along_z, 2, range(1, nz))],
+            (weights.spread, 1, far),
+        ]
     ]
     for zr in sorted(range(1, nz), key=lambda zr: -(zr & -zr)):
         hand_on(zr)
         for item in meanwhile.pop(0) if meanwhile else ():
             each(*item)
+    each(weights.along_z, 2, far)
     for items in meanwhile:
         for item in items:
             each(*item)
-    each(weights.spread, 1, far)
     each(weights.relay, 1, far)
     each(weights.spread, 2, near)
     each(weights.relay, 2, near)

time: 131 us -> 129 us (0.985)
  Pallas kernels: 123 us -> 120 us
    pallas_call x1, Pallas kernels: 123 us -> 120 us  [shards(): pl.pallas_call(functools.partial(layer_kernel, n, nt, nz), out_shape=jax....]
where the time goes in v4:
time: 129 us; the launch traced here: 128 us
  Pallas kernels  120 us (93%)
  local copies, waits for them, and re-layouts  5.54 us (4%)
  other arithmetic  2.69 us (2%)
    pallas_call x1, Pallas kernels, shards(): pl.pallas_call(functools.partial(layer_kernel, n, nt, nz), out_shape=jax....  120 us

profile of v4, /device:TPU:0, one launch (start us, length us, event | category | flops | bytes accessed | tf_op | source)
XLA Modules:
  0.0 128.5 jit_solution(13391860793737432984)
XLA Ops:
  0.0 0.0 copy-start.1
  0.0 0.0 copy-start
  0.0 0.7 exp.6
  0.7 1.0 fusion.1
  1.7 0.1 stack.33
  1.8 0.1 stack.34
  1.8 0.1 stack.35
  1.9 0.1 stack.36
  2.0 0.6 pad_maximum_fusion.lines
  2.6 1.1 maximum_bitcast_fusion
  3.7 0.2 copy.18
  3.9 0.0 copy-start.2
  3.9 0.9 reshape.25.entry
  4.8 0.0 copy-done.1
  4.8 0.0 copy-done
  4.8 0.2 copy.19
  5.0 0.9 reshape.26.read
  5.9 0.0 copy-done.2
  5.9 0.7 copy.20.added
  6.6 120.2 %shard_map.163 = bf16[64,2048]{1,0:T(8,128)(2,1)} custom-call(bf16[256,512]{1,0:T(8,128)(2,1)} %u.1, f32[256,32]{1,0:T(8,128)} %copy.20.added, f32[4,2048]{1,0:T(4,128)} %pad_maximum_fusion.lines, f32[2,16,2048]{2,1,0:T(8,128)} %reshape.25.entry, f32[2,16,2048]{2,1,0:T(8,128)} %reshape.26.read, bf16[64,2048]{1,0:T(8,128)(2,1)} %residual.1, ...), custom_call_target="tpu_custom_call" | custom-call | tf_op jit(solution)/shard_map/pallas_call | solution.py:734
  126.8 1.7 %copy.22 = bf16[64,2048]{1,0:T(8,128)(2,1)} copy(bf16[64,2048]{1,0:T(8,128)(2,1)} %shard_map.163) | data formatting | bytes 524288
  (1 shorter events, 0.0 us)
Async XLA Ops:
  0.0 4.8 %copy-start.1 = (f32[32,16,64]{2,1,0:T(8,128)S(1)}, f32[32,16,64]{2,1,0:T(8,128)}, u32[]{:S(2)}) copy-start(f32[32,16,64]{2,1,0:T(8,128)} %param.24) | copy-start | bytes 393220
  0.0 4.8 %copy-start = (f32[32,16,64]{2,1,0:T(8,128)S(1)}, f32[32,16,64]{2,1,0:T(8,128)}, u32[]{:S(2)}) copy-start(f32[32,16,64]{2,1,0:T(8,128)} %param.25) | copy-start | bytes 393220
  3.9 2.0 %copy-start.2 = (f32[256,32]{0,1:T(8,128)S(1)}, f32[256,32]{0,1:T(8,128)}, u32[]{:S(2)}) copy-start(f32[256,32]{0,1:T(8,128)} %param.26) | copy-start | bytes 98308
